TPU v7x, 128 devices: a whole 4x4x4 slice. The times are simulated.
128 devices in a mesh: rep: 16 (over z, x), fs: 4 (over y), tp: 2 (over core).
Axes of the slice: x: 4, y: 4, z: 4, core: 2. Of those that a mesh axis runs over, the one named last changes fastest.
Arguments:
- inputs: bfloat16 [64, 768, 2048], P(('rep', 'fs'), 'tp'), may hold values from -6 to 6
- pre_gate: bfloat16 [64, 768, 2816], P(('rep', 'fs'), None, 'tp'), may hold values from -6 to 6
- pre_up: bfloat16 [64, 768, 2816], P(('rep', 'fs'), None, 'tp'), may hold values from -6 to 6
- cotangent: bfloat16 [64, 768, 2816], P(('rep', 'fs'), None, 'tp'), may hold values from -16 to 16
- w_gate: bfloat16 [2048, 2816], P('fs', 'tp'), may hold values from -0.125 to 0.125
- w_up: bfloat16 [2048, 2816], P('fs', 'tp'), may hold values from -0.125 to 0.125
- taps_gate: bfloat16 [3, 2816], replicated, may hold values from -3 to 3
- taps_up: bfloat16 [3, 2816], replicated, may hold values from -3 to 3
Outputs:
- grad_inputs: bfloat16 [64, 768, 2048], P(('rep', 'fs'), 'tp')
- grad_w_gate: float32 [2048, 2816], P('fs', 'tp')
- grad_w_up: float32 [2048, 2816], P('fs', 'tp')
- grad_taps_gate: float32 [3, 2816], replicated
- grad_taps_up: float32 [3, 2816], replicated
All inputs are finite; a program needn't handle non-finite values.
Results may differ from a plain program's by a relative error of at most 0.0059.
Values may be sent and summed in bfloat16 or wider, within the bound.
No kernel may reach another device: no remote copies, remote signals or barrier semaphores. Data moves between devices by JAX's collectives and lax.ppermute only.
A program may use at most 192 MiB of HBM per device.

v0:
```python
import jax
import jax.numpy as jnp
from jax import lax
from jax.sharding import PartitionSpec as P


def laid_out(parts, dim):
    lengths = list(parts.shape[1:])
    lengths[dim] *= parts.shape[0]
    return jnp.moveaxis(parts, 0, dim).reshape(lengths)


def work_in_pieces(x, axis, dim, apply, out_dim):
    size, width = (lax.axis_size(axis), x.shape[dim])
    count = 2 if width % 2 == 0 else 1
    gathered, length = ([], width // count)
    for k in range(count):
        section = lax.slice_in_dim(x, k * length, (k + 1) * length, axis=dim)
        starts = jnp.arange(size) * width + k * length
        gathered.append(jax.vmap(apply)(lax.all_gather(section, axis), starts))
    return laid_out(jnp.concatenate(gathered, axis=out_dim + 1), out_dim)


def split_up(x, dim, count):
    before, after = (x.shape[:dim], x.shape[dim + 1 :])
    return jnp.moveaxis(x.reshape(*before, count, -1, *after), dim, 0)


def sum_at_owner(x, axis, dim):
    count = lax.axis_size(axis)
    parts = lax.all_to_all(split_up(x, dim, count), axis, 0, 0, tiled=True)
    return jnp.sum(parts.astype(jnp.float32), axis=0)


def side_by_side(arrays, axis, dim, along):
    widths = [a.shape[along] for a in arrays]
    both = jnp.concatenate(arrays, axis=along)
    result = lax.psum_scatter(both, axis, scatter_dimension=dim, tiled=True)
    return tuple(jnp.split(result, [sum(widths[:k]) for k in range(1, len(widths))], axis=along))


def in_one(arrays, axis):
    ravelled, at, gathered = (jnp.concatenate([a.reshape(-1) for a in arrays]), 0, [])
    subtotal = lax.psum(ravelled, axis)
    for a in arrays:
        gathered.append(subtotal[at : at + a.size].reshape(a.shape))
        at += a.size
    return tuple(gathered)


def causal_mix(signal, kernel):
    length = signal.shape[0]
    padded = jnp.pad(signal, ((2, 0), (0, 0)))
    return (
        kernel[0] * padded[0:length]
        + kernel[1] * padded[1 : length + 1]
        + kernel[2] * padded[2 : length + 2]
    )


def gated_hidden(gate_pre, up_pre, kernel_gate, kernel_up):
    return jax.nn.gelu(causal_mix(gate_pre, kernel_gate)) * causal_mix(up_pre, kernel_up)


def per_device(inputs, pre_gate, pre_up, cotangent, w_gate, w_up, taps_gate, taps_up):
    columns = pre_gate.shape[2]
    offset = lax.axis_index("tp") * columns
    kernel_gate = lax.dynamic_slice_in_dim(taps_gate, offset, columns, 1).astype(jnp.float32)
    kernel_up = lax.dynamic_slice_in_dim(taps_up, offset, columns, 1).astype(jnp.float32)
    _, pullback = jax.vjp(
        gated_hidden,
        pre_gate[0].astype(jnp.float32),
        pre_up[0].astype(jnp.float32),
        kernel_gate,
        kernel_up,
    )
    back_gate, back_up, tap_gate, tap_up = pullback(cotangent[0].astype(jnp.float32))
    stacked = jnp.stack([back_gate, back_up], axis=1).astype(jnp.bfloat16)
    weights = jnp.stack([w_gate, w_up])

    def project(weight_block, row_start):
        return jnp.einsum("lkf,knf->ln", stacked, weight_block, preferred_element_type=jnp.float32)

    partial_value = work_in_pieces(weights, "fs", 1, project, 1)
    grad_inputs = sum_at_owner(partial_value.astype(jnp.bfloat16), "tp", 0).astype(jnp.bfloat16)[
        None
    ]
    rep_count = lax.axis_size("rep")
    shard_count = lax.axis_size("fs")
    features = inputs.shape[2]
    layout = (shard_count, features // shard_count)
    pattern = "nfd,nk->fdk"
    token_block = lax.all_gather(inputs, "tp", axis=1, tiled=True)
    row_count = token_block.shape[1]
    spread = token_block[0].reshape((row_count,) + layout)
    gate_total = jnp.einsum(pattern, spread, stacked[:, 0], preferred_element_type=jnp.float32)
    up_total = jnp.einsum(pattern, spread, stacked[:, 1], preferred_element_type=jnp.float32)
    factor = float(pre_gate.shape[1] * rep_count * shard_count) ** (-0.5)
    pieces = side_by_side((gate_total, up_total), "fs", 0, 1)
    whole = lax.psum((pieces[0], pieces[1]), "rep")
    grad_w_gate = whole[0].reshape(features // shard_count, columns) * factor
    grad_w_up = whole[1].reshape(features // shard_count, columns) * factor
    blank = jnp.zeros(taps_gate.shape, jnp.float32)
    full_gate = lax.dynamic_update_slice_in_dim(blank, tap_gate, offset, 1)
    full_up = lax.dynamic_update_slice_in_dim(blank, tap_up, offset, 1)
    summed_gate, summed_up = in_one((full_gate, full_up), ("rep", "fs", "tp"))
    return (grad_inputs, grad_w_gate, grad_w_up, summed_gate * factor, summed_up * factor)


def solution(mesh):
    placed = (
        P(("rep", "fs"), "tp", None),
        P(("rep", "fs"), None, "tp"),
        P(("rep", "fs"), None, "tp"),
        P(("rep", "fs"), None, "tp"),
        P("fs", "tp"),
        P("fs", "tp"),
        P(),
        P(),
    )
    return jax.shard_map(
        per_device,
        mesh=mesh,
        in_specs=placed,
        out_specs=(P(("rep", "fs"), "tp", None), P("fs", "tp"), P("fs", "tp"), P(), P()),
        check_vma=False,
    )
```

profile of v0, /device:TPU:1, one launch (start us, length us, event | category | flops | bytes accessed | tf_op | source)
XLA Modules:
  0.0 535.5 jit_solution(3696512987416850347)
XLA Ops:
  8.0 0.0 all-gather.6.cloned.1.call-start
  8.0 0.7 all-gather.6.cloned.1.call-update
  8.7 0.0 reduce-scatter.2.cloned.1.call-start
  8.8 0.7 dynamic-slice_convert_fusion
  9.6 0.1 slice_reduce_fusion.5
  9.6 0.0 copy-start
  9.6 0.0 copy-start.2
  9.6 3.0 bitcast_convert_fusion.2
  12.6 0.0 copy-done
  12.6 0.6 copy-done.2
  13.2 0.0 copy-start.1
  13.2 7.1 %multiply_reduce_fusion.4 = (f32[1408]{0:T(1024)S(1)}, f32[1408]{0:T(1024)S(1)}, f32[1408]{0:T(1024)S(1)}, f32[768,1408]{1,0:T(8,128)S(1)}, f32[768,1408]{1,0:T(8,128)S(1)}) fusion(f32[768,1408]{1,0:T(8,128)S(1)} %get-tuple-element.41, bf16[1,768,1408]{2,1,0:T(8,128)(2,1)S(1)} %copy-done, f32[768,1408]{1,0:T(8,128)S(1)} %get-tuple-element.42, ...), kind=kLoop, calls=%fused_computation.24 | loop fusion | flops 41086848 | bytes 21677568 | tf_op jit(solution)/shard_map/transpose(jvp())/reduce_sum | solution.py:56
  20.3 0.0 copy-done.1
  20.3 4.6 multiply_reduce_fusion.1
  25.0 2.8 broadcast_multiply_fusion.2
  27.8 4.8 fusion.6
  32.6 0.8 broadcast_multiply_fusion.5
  33.4 2.3 fusion.7
  35.8 0.0 all-gather.6.cloned.1.call-done
  35.8 3.4 copy.16
  39.2 0.0 copy-start.5
  39.2 7.3 %convolution_bitcast_fusion = f32[4,512,1408]{2,1,0:T(8,128)S(1)} fusion(bf16[768,4,512]{0,2,1:T(8,128)(2,1)S(1)} %bitcast.73, bf16[768,1408]{1,0:T(8,128)(2,1)} %fusion.6), kind=kOutput, calls=%fused_computation.1 | convolution fusion | flops 4429185024 | bytes 16842752 | tf_op jit(solution)/shard_map/nfd,nk->fdk/dot_general | solution.py:97
  46.5 0.0 copy-done.5
  46.5 5.5 %convolution_bitcast_fusion.1 = f32[4,512,1408]{2,1,0:T(8,128)S(1)} fusion(bf16[768,4,512]{0,2,1:T(8,128)(2,1)S(1)} %bitcast.74, bf16[768,1408]{1,0:T(8,128)(2,1)S(1)} %copy-done.5), kind=kOutput, calls=%fused_computation.2 | convolution fusion | flops 4429185024 | bytes 16842752 | tf_op jit(solution)/shard_map/nfd,nk->fdk/dot_general | solution.py:96
  52.0 9.1 %pad_maximum_fusion = f32[4,1024,1408]{2,1,0:T(8,128)} fusion(f32[4,512,1408]{2,1,0:T(8,128)S(1)} %convolution_bitcast_fusion, f32[4,512,1408]{2,1,0:T(8,128)S(1)} %convolution_bitcast_fusion.1), kind=kLoop, calls=%fused_computation | loop fusion | flops 5767168 | bytes 46137344 | tf_op jit(solution)/shard_map/concatenate | solution.py:37
  61.1 0.0 copy-start.7
  61.1 0.0 copy-start.8
  61.1 0.0 reduce-scatter.2.cloned.1.call-update
  61.2 0.0 all-reduce.18.cloned.1.call-start
  61.4 0.6 pad_maximum_fusion.2
  62.1 0.0 all-reduce.18.cloned.1.call-update
  62.1 0.0 all-gather.10.cloned.1.call-start
  62.2 0.4 copy-done.7
  62.5 0.4 copy-done.8
  62.9 1.8 fusion.14
  64.7 0.0 all-gather.10.cloned.1.call-update
  64.8 0.0 all-gather.8.cloned.1.call-start
  64.8 0.5 all-gather.8.cloned.1.call-update
  65.3 0.3 all-reduce.20.cloned.1.call-start
  65.6 198.4 %reduce-scatter.2.cloned.1.call-done = f32[1,1024,1408]{2,1,0:T(8,128)} async-done(((f32[4,1024,1408]{2,1,0:T(8,128)}), f32[1,1024,1408]{2,1,0:T(8,128)}) %reduce-scatter.2.cloned.1.call-update) | async-done | bytes 5767184 | tf_op jit(solution)/shard_map/reduce_scatter | solution.py:38
  264.0 5.6 %fusion.18 = (f32[1,512,1408]{2,1,0:T(8,128)}, f32[1,512,1408]{2,1,0:T(8,128)}) fusion(f32[1,1024,1408]{2,1,0:T(8,128)} %reduce-scatter.2.cloned.1.call-done), kind=kLoop, calls=%fused_computation.69 | loop fusion | bytes 11534336 | tf_op jit(solution)/shard_map/split | solution.py:39
  269.6 0.0 copy-start.4
  269.6 0.0 all-reduce.20.cloned.1.call-update
  269.6 134.9 %all-reduce.18.cloned.1.call-done = f32[16896]{0:T(1024)} async-done(((f32[16896]{0:T(1024)}), f32[16896]{0:T(1024)}) %all-reduce.18.cloned.1.call-update) | async-done | bytes 67600 | tf_op jit(solution)/shard_map/psum | solution.py:44
  404.5 0.9 slice_multiply_fusion
  405.4 0.6 mul.244
  406.0 0.6 mul.246
  406.6 0.0 copy-done.4
  406.6 9.1 %fusion.13 = bf16[4,768,256]{1,2,0:T(8,128)(2,1)} fusion(bf16[4,2,256,1408]{3,2,1,0:T(8,128)(2,1)} %bitcast.81, bf16[768,1,1408]{2,0,1:T(8,128)(2,1)S(1)} %bitcast.75, bf16[768,1,1408]{2,0,1:T(8,128)(2,1)} %bitcast.77), kind=kOutput, calls=%fused_computation.51 | convolution fusion | flops 4438622208 | bytes 11665408 | tf_op jit(solution)/shard_map/vmap(lkf,knf->ln)/dot_general | solution.py:82
  415.7 0.0 all-gather.8.cloned.1.call-done
  415.7 0.0 copy-start.6
  415.7 8.1 %fusion.12 = bf16[4,768,256]{1,2,0:T(8,128)(2,1)S(1)} fusion(bf16[4,2,256,1408]{3,2,1,0:T(8,128)(2,1)} %bitcast.82, bf16[768,1,1408]{2,0,1:T(8,128)(2,1)S(1)} %bitcast.76, bf16[768,1,1408]{2,0,1:T(8,128)(2,1)} %bitcast.78), kind=kOutput, calls=%fused_computation.50 | convolution fusion | flops 4438622208 | bytes 11665408 | tf_op jit(solution)/shard_map/vmap(lkf,knf->ln)/dot_general | solution.py:82
  423.8 0.0 copy-done.6
  423.8 0.2 maximum_bitcast_fusion.1
  424.0 2.4 convert_element_type.47
  426.5 2.3 copy.14
  428.8 5.9 %all_to_all.5 = bf16[2,384,2048]{1,2,0:T(8,128)(2,1)S(1)} all-to-all(bf16[2,384,2048]{1,2,0:T(8,128)(2,1)S(1)} %copy.14), channel_id=1, replica_groups=mesh['rep'=16,'fs'=4,'tp'=2] {'tp'}, dimensions={0} | all-to-all | bytes 6291456 | tf_op jit(solution)/shard_map/all_to_all | solution.py:31
  434.7 2.2 reduce_sum.65
  436.8 2.6 copy.17
  439.4 83.4 %all-reduce.20.cloned.1.call-done = (f32[1,512,1408]{2,1,0:T(8,128)}, f32[1,512,1408]{2,1,0:T(8,128)}) async-done(((f32[1,512,1408]{2,1,0:T(8,128)}, f32[1,512,1408]{2,1,0:T(8,128)}), (f32[1,512,1408]{2,1,0:T(8,128)}, f32[1,512,1408]{2,1,0:T(8,128)})) %all-reduce.20.cloned.1.call-update) | async-done | bytes 5767184 | tf_op jit(solution)/shard_map/psum | solution.py:100
  522.8 0.0 copy-start.3
  522.8 3.8 multiply_bitcast_fusion.1
  526.6 0.0 copy-done.3
  526.6 1.8 multiply_bitcast_fusion
  (14 shorter events, 0.2 us)
Async XLA Ops:
  8.0 27.8 %all-gather.6.cloned.1.call-start = ((), (), s32[]{:S(2)}) async-start(), calls=%async_computation.2 | async-start | bytes 4718592 | tf_op jit(solution)/shard_map/all_gather | solution.py:93
  8.7 255.2 %reduce-scatter.2.cloned.1.call-start = ((), (), s32[]{:S(2)}) async-start(), calls=%async_computation.3 | async-start | bytes 28835840 | tf_op jit(solution)/shard_map/reduce_scatter | solution.py:38
  9.6 3.0 copy-start
  9.6 3.6 copy-start.2
  13.2 7.1 %copy-start.1 = (bf16[1,768,1408]{2,1,0:T(8,128)(2,1)S(1)}, bf16[1,768,1408]{2,1,0:T(8,128)(2,1)}, u32[]{:S(2)}) copy-start(bf16[1,768,1408]{2,1,0:T(8,128)(2,1)} %param.10) | copy-start | bytes 6488068
  39.2 7.3 %copy-start.5 = (bf16[768,1408]{1,0:T(8,128)(2,1)S(1)}, bf16[768,1408]{1,0:T(8,128)(2,1)}, u32[]{:S(2)}) copy-start(bf16[768,1408]{1,0:T(8,128)(2,1)} %fusion.7) | copy-start | bytes 6488068
  61.1 1.4 copy-start.7
  61.1 1.8 copy-start.8
  61.2 343.4 %all-reduce.18.cloned.1.call-start = ((), (), s32[]{:S(2)}) async-start(), calls=%async_computation.4 | async-start | bytes 139264 | tf_op jit(solution)/shard_map/psum | solution.py:44
  62.1 344.5 %all-gather.10.cloned.1.call-start = ((), (), s32[]{:S(2)}) async-start(), calls=%async_computation.6 | async-start | bytes 7208960 | tf_op jit(solution)/shard_map/all_gather | solution.py:20
  64.8 351.0 %all-gather.8.cloned.1.call-start = ((), (), s32[]{:S(2)}) async-start(), calls=%async_computation.5 | async-start | bytes 7208960 | tf_op jit(solution)/shard_map/all_gather | solution.py:20
  65.3 457.5 %all-reduce.20.cloned.1.call-start = ((), (), s32[]{:S(2)}) async-start(), calls=%async_computation.7 | async-start | bytes 11534336 | tf_op jit(solution)/shard_map/psum | solution.py:100
  269.6 137.1 %copy-start.4 = (bf16[768,1408]{1,0:T(8,128)(2,1)S(1)}, bf16[768,1408]{1,0:T(8,128)(2,1)}, u32[]{:S(2)}) copy-start(bf16[768,1408]{1,0:T(8,128)(2,1)} %fusion.6) | copy-start | bytes 6488068
  415.7 8.1 %copy-start.6 = (bf16[4,768,256]{1,2,0:T(8,128)(2,1)S(1)}, bf16[4,768,256]{1,2,0:T(8,128)(2,1)}, u32[]{:S(2)}) copy-start(bf16[4,768,256]{1,2,0:T(8,128)(2,1)} %fusion.13) | copy-start | bytes 4718596
  522.8 3.8 copy-start.3
Sparse Core Ops, SparseCore 0:
  10.5 18.4 all-gather.5
  61.3 202.6 reduce-scatter.1
  266.2 60.8 all-gather.9
  328.6 61.9 all-gather.7
Sparse Core Ops, SparseCore 1:
  66.4 338.1 all-reduce.17
  408.4 114.3 all-reduce.19
where the time goes:
time: 536 us
  waiting for transfers between devices  418 us (78%)
  other arithmetic  46.8 us (9%)
  matrix products  29.9 us (6%)
  local copies, waits for them, and re-layouts  19.1 us (4%)
  between operations  15.4 us (3%)
  blocking collectives  5.9 us (1%)
    reduce_scatter x1, waiting for transfers between devices, side_by_side(): result = lax.psum_scatter(both, axis, scatter_dimension=dim, tiled=True)  198 us
    psum x1, waiting for transfers between devices, in_one(): subtotal = lax.psum(ravelled, axis)  135 us
    psum x1, waiting for transfers between devices, per_device(): whole = lax.psum((pieces[0], pieces[1]), 'rep')  83.4 us
    dot_general x2, matrix products, project(): jnp.einsum('lkf,knf->ln', stacked, weight_block, preferred_element_type=j...  17.1 us
    reduce_sum x2, other arithmetic, causal_mix(): kernel[1] * padded[1:length + 1]  11.8 us
  transfers between devices with their start and end apart: 6, of which 3 were waited for; matrix products, arithmetic and copies ran while one was open for 12% of the time, Pallas kernels for 0%

commit v1 on v0

--- a/solution.py
+++ b/solution.py
@@ -2,6 +2,7 @@
 import jax.numpy as jnp
 from jax import lax
 from jax.sharding import PartitionSpec as P
+from jax.lax import all_gather
 
 
 def laid_out(parts, dim):
@@ -41,7 +42,7 @@
 
 def in_one(arrays, axis):
     ravelled, at, gathered = (jnp.concatenate([a.reshape(-1) for a in arrays]), 0, [])
-    subtotal = lax.psum(ravelled, axis)
+    subtotal = jnp.sum(all_gather(ravelled, axis), axis=0)
     for a in arrays:
         gathered.append(subtotal[at : at + a.size].reshape(a.shape))
         at += a.size

time: 536 us -> 594 us (1.11)
  waiting for transfers between devices: 418 us -> 470 us
    psum x1 -> x0, waiting for transfers between devices: 135 us -> none  [in_one(): subtotal = lax.psum(ravelled, axis)]
    all_gather x2, waiting for transfers between devices: 0.01 us -> 112 us  [work_in_pieces(): gathered.append(jax.vmap(apply)(lax.all_gather(section, axis), starts))]
    all_gather x0 -> x1, waiting for transfers between devices: none -> 49.2 us  [in_one(): subtotal = jnp.sum(all_gather(ravelled, axis), axis=0)]
    psum x1, waiting for transfers between devices: 83.4 us -> 111 us  [per_device(): whole = lax.psum((pieces[0], pieces[1]), 'rep')]
    reduce_sum x0 -> x1, other arithmetic: none -> 6.5 us  [in_one(): subtotal = jnp.sum(all_gather(ravelled, axis), axis=0)]
  transfers between devices with their start and end apart: 6 -> 6, of which waited for: 3 -> 5; matrix products, arithmetic and copies ran while one was open for 12% -> 12% of each run, Pallas kernels for 0% -> 0%
where the time goes in v1:
time: 594 us
  waiting for transfers between devices  470 us (79%)
  other arithmetic  51.7 us (9%)
  matrix products  29.9 us (5%)
  local copies, waits for them, and re-layouts  20.7 us (3%)
  between operations  14.4 us (2%)
  blocking collectives  6.72 us (1%)
    reduce_scatter x1, waiting for transfers between devices, side_by_side(): result = lax.psum_scatter(both, axis, scatter_dimension=dim, tiled=True)  197 us
    all_gather x2, waiting for transfers between devices, work_in_pieces(): gathered.append(jax.vmap(apply)(lax.all_gather(section, axis), starts))  112 us
    psum x1, waiting for transfers between devices, per_device(): whole = lax.psum((pieces[0], pieces[1]), 'rep')  111 us
    all_gather x1, waiting for transfers between devices, in_one(): subtotal = jnp.sum(all_gather(ravelled, axis), axis=0)  49.2 us
    dot_general x2, matrix products, project(): jnp.einsum('lkf,knf->ln', stacked, weight_block, preferred_element_type=j...  17.1 us
  transfers between devices with their start and end apart: 6, of which 5 were waited for; matrix products, arithmetic and copies ran while one was open for 12% of the time, Pallas kernels for 0%

profile of v1, /device:TPU:1, one launch (start us, length us, event | category | flops | bytes accessed | tf_op | source)
XLA Modules:
  0.0 593.6 jit_solution(15698841519979893899)
XLA Ops:
  7.2 0.0 all-gather.9.cloned.1.call-start
  7.2 0.7 all-gather.9.cloned.1.call-update
  7.9 0.0 reduce-scatter.2.cloned.1.call-start
  8.0 0.7 dynamic-slice_convert_fusion
  8.7 0.1 slice_reduce_fusion.5
  8.8 0.0 copy-start
  8.8 0.0 copy-start.2
  8.8 3.0 bitcast_convert_fusion.2
  11.8 0.0 copy-done
  11.8 0.6 copy-done.2
  12.4 0.0 copy-start.1
  12.4 7.1 %multiply_reduce_fusion.4 = (f32[1408]{0:T(1024)S(1)}, f32[1408]{0:T(1024)S(1)}, f32[1408]{0:T(1024)S(1)}, f32[768,1408]{1,0:T(8,128)S(1)}, f32[768,1408]{1,0:T(8,128)S(1)}) fusion(f32[768,1408]{1,0:T(8,128)S(1)} %get-tuple-element.41, bf16[1,768,1408]{2,1,0:T(8,128)(2,1)S(1)} %copy-done, f32[768,1408]{1,0:T(8,128)S(1)} %get-tuple-element.42, ...), kind=kLoop, calls=%fused_computation.24 | loop fusion | flops 41086848 | bytes 21677568 | tf_op jit(solution)/shard_map/transpose(jvp())/reduce_sum | solution.py:57
  19.5 0.0 copy-done.1
  19.5 4.6 multiply_reduce_fusion.1
  24.2 2.8 broadcast_multiply_fusion.2
  27.0 4.7 fusion.6
  31.7 0.8 broadcast_multiply_fusion.5
  32.6 2.3 fusion.7
  34.9 0.0 all-gather.9.cloned.1.call-done
  34.9 3.4 copy.16
  38.3 0.0 copy-start.5
  38.3 7.3 %convolution_bitcast_fusion = f32[4,512,1408]{2,1,0:T(8,128)S(1)} fusion(bf16[768,4,512]{0,2,1:T(8,128)(2,1)S(1)} %bitcast.73, bf16[768,1408]{1,0:T(8,128)(2,1)} %fusion.6), kind=kOutput, calls=%fused_computation.1 | convolution fusion | flops 4429185024 | bytes 16842752 | tf_op jit(solution)/shard_map/nfd,nk->fdk/dot_general | solution.py:98
  45.6 0.0 copy-done.5
  45.6 5.5 convolution_bitcast_fusion.1
  51.1 9.1 %pad_maximum_fusion = f32[4,1024,1408]{2,1,0:T(8,128)} fusion(f32[4,512,1408]{2,1,0:T(8,128)S(1)} %convolution_bitcast_fusion, f32[4,512,1408]{2,1,0:T(8,128)S(1)} %convolution_bitcast_fusion.1), kind=kLoop, calls=%fused_computation | loop fusion | flops 5767168 | bytes 46137344 | tf_op jit(solution)/shard_map/concatenate | solution.py:38
  60.2 0.0 copy-start.7
  60.2 0.0 copy-start.8
  60.2 0.0 reduce-scatter.2.cloned.1.call-update
  60.3 0.0 all-gather.13.cloned.1.call-start
  60.3 1.3 copy-done.7
  61.6 0.4 copy-done.8
  62.0 1.8 fusion.14
  63.8 0.0 all-gather.13.cloned.1.call-update
  63.8 0.0 all-gather.11.cloned.1.call-start
  63.9 0.5 all-gather.11.cloned.1.call-update
  64.4 0.0 all-gather.15.cloned.1.call-start
  64.7 0.7 reshape.100
  65.4 0.0 all-gather.15.cloned.1.call-update
  65.4 0.3 all-reduce.17.cloned.1.call-start
  65.7 196.7 %reduce-scatter.2.cloned.1.call-done = f32[1,1024,1408]{2,1,0:T(8,128)} async-done(((f32[4,1024,1408]{2,1,0:T(8,128)}), f32[1,1024,1408]{2,1,0:T(8,128)}) %reduce-scatter.2.cloned.1.call-update) | async-done | bytes 5767184 | tf_op jit(solution)/shard_map/reduce_scatter | solution.py:39
  262.4 5.6 fusion.18
  268.0 0.0 copy-start.4
  268.0 0.0 all-reduce.17.cloned.1.call-update
  268.0 57.6 %all-gather.13.cloned.1.call-done = bf16[8,256,1408]{2,1,0:T(8,128)(2,1)} async-done(((bf16[2,256,1408]{2,1,0:T(8,128)(2,1)}), bf16[8,256,1408]{2,1,0:T(8,128)(2,1)}) %all-gather.13.cloned.1.call-update) | async-done | bytes 5767184 | tf_op jit(solution)/shard_map/all_gather | solution.py:21
  325.5 0.0 copy-done.4
  325.5 9.1 %fusion.13 = bf16[4,768,256]{1,2,0:T(8,128)(2,1)} fusion(bf16[4,2,256,1408]{3,2,1,0:T(8,128)(2,1)} %bitcast.81, bf16[768,1,1408]{2,0,1:T(8,128)(2,1)S(1)} %bitcast.75, bf16[768,1,1408]{2,0,1:T(8,128)(2,1)} %bitcast.77), kind=kOutput, calls=%fused_computation.51 | convolution fusion | flops 4438622208 | bytes 11665408 | tf_op jit(solution)/shard_map/vmap(lkf,knf->ln)/dot_general | solution.py:83
  334.6 54.3 %all-gather.11.cloned.1.call-done = bf16[8,256,1408]{2,1,0:T(8,128)(2,1)} async-done(((bf16[2,256,1408]{2,1,0:T(8,128)(2,1)}), bf16[8,256,1408]{2,1,0:T(8,128)(2,1)}) %all-gather.11.cloned.1.call-update) | async-done | bytes 5767184 | tf_op jit(solution)/shard_map/all_gather | solution.py:21
  388.9 0.0 copy-start.6
  388.9 8.1 %fusion.12 = bf16[4,768,256]{1,2,0:T(8,128)(2,1)S(1)} fusion(bf16[4,2,256,1408]{3,2,1,0:T(8,128)(2,1)} %bitcast.82, bf16[768,1,1408]{2,0,1:T(8,128)(2,1)S(1)} %bitcast.76, bf16[768,1,1408]{2,0,1:T(8,128)(2,1)} %bitcast.78), kind=kOutput, calls=%fused_computation.50 | convolution fusion | flops 4438622208 | bytes 11665408 | tf_op jit(solution)/shard_map/vmap(lkf,knf->ln)/dot_general | solution.py:83
  397.0 0.0 copy-done.6
  397.0 0.2 maximum_bitcast_fusion.1
  397.2 2.4 convert_element_type.47
  399.7 2.3 copy.14
  401.9 6.7 %all_to_all.5 = bf16[2,384,2048]{1,2,0:T(8,128)(2,1)S(1)} all-to-all(bf16[2,384,2048]{1,2,0:T(8,128)(2,1)S(1)} %copy.14), channel_id=1, replica_groups=mesh['rep'=16,'fs'=4,'tp'=2] {'tp'}, dimensions={0} | all-to-all | bytes 6291456 | tf_op jit(solution)/shard_map/all_to_all | solution.py:32
  408.7 2.2 reduce_sum.76
  410.8 2.6 copy.17
  413.4 49.2 %all-gather.15.cloned.1.call-done = f32[128,1,16896]{2,1,0:T(1,128)} async-done(((f32[1,1,16896]{2,1,0:T(1,128)}), f32[128,1,16896]{2,1,0:T(1,128)}) %all-gather.15.cloned.1.call-update) | async-done | bytes 8650768 | tf_op jit(solution)/shard_map/all_gather | solution.py:45
  462.6 6.5 %reduce_sum.86 = f32[16896]{0:T(1024)S(1)} reduce(f32[128,1,16896]{2,1,0:T(1,128)} %all-gather.15.cloned.1.call-done, f32[]{:T(128)} %constant.8.clone.1), dimensions={0,1}, to_apply=%region_10.11 | reduce | flops 2145792 | bytes 8718340 | tf_op jit(solution)/shard_map/reduce_sum | solution.py:45
  469.1 0.6 mul.244
  469.8 0.6 mul.246
  470.4 110.8 %all-reduce.17.cloned.1.call-done = (f32[1,512,1408]{2,1,0:T(8,128)}, f32[1,512,1408]{2,1,0:T(8,128)}) async-done(((f32[1,512,1408]{2,1,0:T(8,128)}, f32[1,512,1408]{2,1,0:T(8,128)}), (f32[1,512,1408]{2,1,0:T(8,128)}, f32[1,512,1408]{2,1,0:T(8,128)})) %all-reduce.17.cloned.1.call-update) | async-done | bytes 5767184 | tf_op jit(solution)/shard_map/psum | solution.py:101
  581.2 3.8 multiply_bitcast_fusion.1
  585.0 0.0 copy-done.3
  585.0 1.8 multiply_bitcast_fusion
  (16 shorter events, 0.2 us)
Async XLA Ops:
  7.2 27.7 %all-gather.9.cloned.1.call-start = ((), (), s32[]{:S(2)}) async-start(), calls=%async_computation.2 | async-start | bytes 4718592 | tf_op jit(solution)/shard_map/all_gather | solution.py:94
  7.9 254.5 %reduce-scatter.2.cloned.1.call-start = ((), (), s32[]{:S(2)}) async-start(), calls=%async_computation.3 | async-start | bytes 28835840 | tf_op jit(solution)/shard_map/reduce_scatter | solution.py:39
  8.8 3.0 copy-start
  8.8 3.6 copy-start.2
  12.4 7.1 %copy-start.1 = (bf16[1,768,1408]{2,1,0:T(8,128)(2,1)S(1)}, bf16[1,768,1408]{2,1,0:T(8,128)(2,1)}, u32[]{:S(2)}) copy-start(bf16[1,768,1408]{2,1,0:T(8,128)(2,1)} %param.10) | copy-start | bytes 6488068
  38.3 7.3 %copy-start.5 = (bf16[768,1408]{1,0:T(8,128)(2,1)S(1)}, bf16[768,1408]{1,0:T(8,128)(2,1)}, u32[]{:S(2)}) copy-start(bf16[768,1408]{1,0:T(8,128)(2,1)} %fusion.7) | copy-start | bytes 6488068
  60.2 1.4 copy-start.7
  60.2 1.8 copy-start.8
  60.3 265.3 %all-gather.13.cloned.1.call-start = ((), (), s32[]{:S(2)}) async-start(), calls=%async_computation.5 | async-start | bytes 7208960 | tf_op jit(solution)/shard_map/all_gather | solution.py:21
  63.8 325.1 %all-gather.11.cloned.1.call-start = ((), (), s32[]{:S(2)}) async-start(), calls=%async_computation.4 | async-start | bytes 7208960 | tf_op jit(solution)/shard_map/all_gather | solution.py:21
  64.4 398.2 %all-gather.15.cloned.1.call-start = ((), (), s32[]{:S(2)}) async-start(), calls=%async_computation.6 | async-start | bytes 8718336 | tf_op jit(solution)/shard_map/all_gather | solution.py:45
  65.4 515.7 %all-reduce.17.cloned.1.call-start = ((), (), s32[]{:S(2)}) async-start(), calls=%async_computation.7 | async-start | bytes 11534336 | tf_op jit(solution)/shard_map/psum | solution.py:101
  268.0 57.6 %copy-start.4 = (bf16[768,1408]{1,0:T(8,128)(2,1)S(1)}, bf16[768,1408]{1,0:T(8,128)(2,1)}, u32[]{:S(2)}) copy-start(bf16[768,1408]{1,0:T(8,128)(2,1)} %fusion.6) | copy-start | bytes 6488068
  388.9 8.1 %copy-start.6 = (bf16[4,768,256]{1,2,0:T(8,128)(2,1)S(1)}, bf16[4,768,256]{1,2,0:T(8,128)(2,1)}, u32[]{:S(2)}) copy-start(bf16[4,768,256]{1,2,0:T(8,128)(2,1)} %fusion.13) | copy-start | bytes 4718596
  581.2 3.8 copy-start.3
Sparse Core Ops, SparseCore 0:
  9.6 18.4 all-gather.8
  60.4 201.9 reduce-scatter.1
  264.6 60.8 all-gather.12
  327.1 61.8 all-gather.10
  391.8 70.8 all-gather.14
  466.5 114.6 all-reduce.16
